TPU v7x, 32 devices: a whole 2x2x4 slice. The times are simulated.
32 devices in a mesh: ep: 8 (over z, x), tp: 4 (over y, core).
Axes of the slice: x: 2, y: 2, z: 4, core: 2. Of those that a mesh axis runs over, the one named last changes fastest.
Arguments:
- mix_bgate: bfloat16 [2048, 1024], P('ep', 'tp'), may hold values from -6 to 6
- mix_cgate: bfloat16 [2048, 1024], P('ep', 'tp'), may hold values from -6 to 6
- mix_input: bfloat16 [2048, 1024], P('ep', 'tp'), may hold values from -6 to 6
- conv_taps: float32 [3, 1024], P(None, 'tp'), may hold values from -3.5 to 3.5
- mix_out_w: bfloat16 [1024, 2048], P('tp'), may hold values from -0.1875 to 0.1875
- moe_x: bfloat16 [2048, 2048], P('ep', 'tp'), may hold values from -6 to 6
- moe_gain: float32 [2048], replicated, may hold values from 0.1 to 1.9
- routes: int32 [2048, 2], P('ep'), may hold values from 0 to 7, all different within a row; in each aligned block of 256 rows (0 to 255, 256 to 511, ...) at most 96 rows name the same one
- route_w: float32 [2048, 2], P('ep'), may hold values from 0.2 to 1
- w_gate: bfloat16 [8, 2048, 3584], P('ep', None, 'tp'), may hold values from -0.125 to 0.125
- w_up: bfloat16 [8, 2048, 3584], P('ep', None, 'tp'), may hold values from -0.125 to 0.125
- w_down: bfloat16 [8, 3584, 2048], P('ep', 'tp'), may hold values from -0.09375 to 0.09375
Outputs:
- mixed: bfloat16 [2048, 2048], P(('ep', 'tp'))
- routed: bfloat16 [2048, 2048], P('ep', 'tp')
Inputs may be any that keep to these rules, and one draw needn't show every extreme that they name: `routes`: among the 256 rows of one index of ep, each row names 2 different experts and no expert is named by more than 96 rows; in every draw some expert is named by exactly 96 rows of some index.
All inputs are finite; a program needn't handle non-finite values.
Results may differ from a plain program's by a relative error of at most 0.012.
Values may be sent and summed in bfloat16 or wider, within the bound.
A program may use at most 64 MiB of HBM per device.

v0:
```python
import jax
import jax.numpy as jnp
from jax import lax
from jax.sharding import PartitionSpec as P


def shifted(block, axis, distance):
    devices = range(lax.axis_size(axis))
    route = [(i - distance, i) for i in devices if i - distance in devices]
    return lax.ppermute(block, axis, route)


def rms_rows(values, gain):
    wide = values.astype(jnp.float32)
    scale = lax.rsqrt(jnp.mean(wide * wide, axis=-1, keepdims=True) + 1e-06)
    return (wide * scale * gain).astype(jnp.bfloat16)


def conv_mixer(mix_bgate, mix_cgate, mix_input, conv_taps, mix_out_w):
    length = mix_input.shape[0]
    reach = conv_taps.shape[0] - 1
    tail = jnp.stack([mix_cgate[length - reach :], mix_input[length - reach :]])
    before = shifted(tail, "ep", 1)
    gates_c = jnp.concatenate([before[0], mix_cgate], 0).astype(jnp.float32)
    inputs_h = jnp.concatenate([before[1], mix_input], 0).astype(jnp.float32)
    prod = gates_c * inputs_h
    conv = conv_taps[0] * prod[0:length]
    for j in range(1, reach + 1):
        conv = conv + conv_taps[j] * prod[j : j + length]
    gated = (mix_bgate.astype(jnp.float32) * conv).astype(jnp.bfloat16)
    return lax.psum_scatter(
        jnp.dot(gated, mix_out_w, preferred_element_type=jnp.float32).astype(jnp.bfloat16),
        "tp",
        scatter_dimension=0,
        tiled=True,
    )


def expert_layer(moe_x, moe_gain, routes, route_w, w_gate, w_up, w_down):
    whole = lax.all_gather(moe_x, "tp", axis=1, tiled=True)
    normed = rms_rows(whole, moe_gain)
    ntok, width = normed.shape
    top = routes.shape[1]
    n_ep = lax.axis_size("ep")
    n_tp = lax.axis_size("tp")
    per_dev = w_gate.shape[0]
    experts = per_dev * n_ep
    cap = 4 * ((3 * ntok * top + 8 * experts - 1) // (8 * experts))
    flat = routes.reshape(-1)
    onehot = (flat[:, None] == jnp.arange(experts, dtype=jnp.int32)[None, :]).astype(jnp.int32)
    earlier = jnp.cumsum(onehot, axis=0) - onehot
    slot = jnp.sum(earlier * onehot, axis=1)
    place = flat * cap + slot
    source = (
        jnp.full((experts * cap,), ntok, jnp.int32)
        .at[place]
        .set(jnp.arange(ntok * top, dtype=jnp.int32) // top)
    )
    padded = jnp.concatenate([normed, jnp.zeros((1, width), jnp.bfloat16)], 0)
    outgoing = padded[source].reshape(n_ep, per_dev, cap, width)
    part = cap // n_tp
    mine = lax.dynamic_slice_in_dim(outgoing, lax.axis_index("tp") * part, part, 2)
    landed = lax.all_to_all(mine, "ep", split_axis=0, concat_axis=0, tiled=True)
    arrived = lax.all_gather(landed, "tp", axis=2, tiled=True)
    gate = jnp.einsum("secd,edf->secf", arrived, w_gate, preferred_element_type=jnp.float32)
    upper = jnp.einsum("secd,edf->secf", arrived, w_up, preferred_element_type=jnp.float32)
    hidden = (jax.nn.silu(gate) * upper).astype(jnp.bfloat16)
    down = jnp.einsum("secf,efd->secd", hidden, w_down, preferred_element_type=jnp.float32)
    summed = lax.psum_scatter(down.astype(jnp.bfloat16), "tp", scatter_dimension=3, tiled=True)
    returned = lax.all_to_all(summed, "ep", split_axis=0, concat_axis=0, tiled=True)
    flat_back = returned.reshape(experts * cap, width // n_tp)
    picked = flat_back[place].astype(jnp.float32).reshape(ntok, top, width // n_tp)
    return jnp.sum(picked * route_w[:, :, None], axis=1).astype(jnp.bfloat16)


def body(
    mix_bgate,
    mix_cgate,
    mix_input,
    conv_taps,
    mix_out_w,
    moe_x,
    moe_gain,
    routes,
    route_w,
    w_gate,
    w_up,
    w_down,
):
    mixed = conv_mixer(mix_bgate, mix_cgate, mix_input, conv_taps, mix_out_w)
    routed = expert_layer(moe_x, moe_gain, routes, route_w, w_gate, w_up, w_down)
    return (mixed, routed)


def solution(mesh):
    in_specs = (
        P("ep", "tp"),
        P("ep", "tp"),
        P("ep", "tp"),
        P(None, "tp"),
        P("tp", None),
        P("ep", "tp"),
        P(),
        P("ep", None),
        P("ep", None),
        P("ep", None, "tp"),
        P("ep", None, "tp"),
        P("ep", "tp", None),
    )
    out_specs = (P(("ep", "tp"), None), P("ep", "tp"))
    return jax.shard_map(body, mesh=mesh, in_specs=in_specs, out_specs=out_specs, check_vma=False)
```

profile of v0, /device:TPU:0, one launch (start us, length us, event | category | flops | bytes accessed | tf_op | source)
XLA Modules:
  0.0 185.2 jit_solution(3375936974495529147)
XLA Ops:
  7.2 0.0 copy-start
  7.2 0.0 all-gather.3.cloned.1.call-start
  7.2 0.7 all-gather.3.cloned.1.call-update
  7.9 0.0 all-gather.5.cloned.1.call-start
  8.0 0.8 copy.20
  8.8 0.1 eq.29
  8.9 0.1 eq.25
  9.1 1.1 reduce-window.6
  10.2 0.2 slice_reduce_fusion
  10.5 0.7 broadcast_multiply_fusion
  11.2 0.1 copy.19
  11.3 0.1 mul.110
  11.5 0.1 fusion.43
  11.6 2.4 %scatter_custom_fusion = s32[768]{0:T(1024)S(1)} fusion(s32[512]{0:T(512)S(1)} %bitcast.108, s32[512]{0:T(512)S(1)} %add_select_fusion, s32[]{:T(128)} %constant.40.clone.1), kind=kCustom, calls=%fused_computation.57 | custom fusion | bytes 3076 | tf_op jit(solution)/shard_map/scatter | solution.py:57
  14.1 15.0 %all-gather.3.cloned.1.call-done = bf16[256,2048]{1,0:T(8,128)(2,1)} async-done(((bf16[256,512]{1,0:T(8,128)(2,1)}), bf16[256,2048]{1,0:T(8,128)(2,1)}) %all-gather.3.cloned.1.call-update) | async-done | bytes 1048592 | tf_op jit(solution)/shard_map/all_gather | solution.py:40
  29.0 1.5 fusion.18
  30.6 1.5 fusion.20
  32.1 0.1 concatenate.11
  32.2 4.3 %gather_fusion = bf16[768,2048]{1,0:T(8,128)(2,1)} fusion(bf16[257,2048]{1,0:T(8,128)(2,1)S(1)} %concatenate.11, s32[1024]{0:T(1024)S(1)} %pad_clamp_fusion.1), kind=kCustom, calls=%fused_computation | custom fusion | bytes 6294528 | tf_op jit(solution)/shard_map/gather | solution.py:60
  36.5 1.2 constant_dynamic-slice_fusion
  37.7 25.9 %all_to_all.10 = bf16[8,1,24,2048]{3,2,1,0:T(8,128)(2,1)} all-to-all(bf16[8,1,24,2048]{3,2,1,0:T(8,128)(2,1)S(1)} %constant_dynamic-slice_fusion), channel_id=1, replica_groups=mesh['ep'=8,'tp'=4] {'ep'}, dimensions={0} | all-to-all | bytes 1572864 | tf_op jit(solution)/shard_map/all_to_all | solution.py:63
  63.6 0.0 all-gather.5.cloned.1.call-update
  63.6 0.0 reduce-scatter.5.cloned.1.call-start
  63.7 26.7 %all-gather.5.cloned.1.call-done = bf16[8,1,96,2048]{3,2,0,1:T(8,128)(2,1)} async-done(((bf16[8,1,24,2048]{3,2,0,1:T(8,128)(2,1)}), bf16[8,1,96,2048]{3,2,0,1:T(8,128)(2,1)}) %all-gather.5.cloned.1.call-update) | async-done | bytes 3145744 | tf_op jit(solution)/shard_map/all_gather | solution.py:64
  90.4 8.0 %fusion.4 = f32[8,96,896]{2,1,0:T(8,128)} fusion(bf16[1,2048,896]{2,1,0:T(8,128)(2,1)} %param.21, bf16[8,1,96,2048]{3,2,0,1:T(8,128)(2,1)} %all-gather.5.cloned.1.call-done), kind=kOutput, calls=%fused_computation.7 | convolution fusion | flops 2818572288 | bytes 9568256 | tf_op jit(solution)/shard_map/secd,edf->secf/dot_general | solution.py:65
  98.4 12.1 %fusion.11 = bf16[8,1,96,2048]{3,2,0,1:T(8,128)(2,1)} fusion(bf16[1,896,2048]{2,1,0:T(8,128)(2,1)} %param.23, bf16[1,2048,896]{2,1,0:T(8,128)(2,1)} %param.22, bf16[8,1,96,2048]{3,2,0,1:T(8,128)(2,1)} %all-gather.5.cloned.1.call-done, f32[8,96,896]{2,1,0:T(8,128)} %fusion.4), kind=kOutput, calls=%fused_computation.12 | convolution fusion | flops 5642846208 | bytes 16384000 | tf_op jit(solution)/shard_map/secf,efd->secd/dot_general | solution.py:68
  110.5 0.0 copy-start.3
  110.5 0.0 reduce-scatter.5.cloned.1.call-update
  110.5 0.0 copy-start.5
  110.5 0.0 reduce-scatter.3.cloned.1.call-start
  110.6 0.8 copy-done.1
  111.4 0.1 copy-done.2
  111.5 3.4 %collective-permute-start = (bf16[2,2,256]{2,1,0:T(2,128)(2,1)S(1)}, bf16[2,2,256]{2,1,0:T(2,128)(2,1)S(1)}, u32[]{:S(2)}, u32[]{:S(2)}) collective-permute-start(bf16[2,2,256]{2,1,0:T(2,128)(2,1)S(1)} %pad_maximum_fusion), channel_id=1, source_target_pairs={{0,4},{4,8},{8,12},{12,16},{16,20},{20,24},{24,28},{1,5},{5,9},{9,... | collective-permute-start | bytes 6152 | tf_op jit(solution)/shard_map/ppermute | solution.py:10
  114.9 0.0 copy-done.4
  114.9 1.3 collective-permute-done
  116.2 0.1 convert_multiply_fusion.2
  116.2 0.0 copy-done
  116.2 0.0 copy-done.3
  116.2 1.5 convolution_convert_fusion
  117.7 0.0 reduce-scatter.3.cloned.1.call-update
  117.7 30.7 %reduce-scatter.5.cloned.1.call-done = bf16[8,1,96,512]{3,2,0,1:T(8,128)(2,1)} async-done(((bf16[8,1,96,2048]{3,2,0,1:T(8,128)(2,1)}), bf16[8,1,96,512]{3,2,0,1:T(8,128)(2,1)}) %reduce-scatter.5.cloned.1.call-update) | async-done | bytes 786448 | tf_op jit(solution)/shard_map/reduce_scatter | solution.py:69
  148.4 5.5 %all-to-all-start.1 = ((bf16[8,1,96,512]{3,2,1,0:T(8,128)(2,1)}), bf16[8,1,96,512]{3,2,1,0:T(8,128)(2,1)S(1)}, u32[]{:S(2)}, u32[]{:S(2)}) async-start(bf16[8,1,96,512]{3,2,1,0:T(8,128)(2,1)} %bitcast.107), calls=%async_computation.3 | async-start | bytes 1572864 | tf_op jit(solution)/shard_map/all_to_all | solution.py:70
  153.9 0.0 copy-done.5
  153.9 0.1 copy.25
  154.1 19.9 %all-to-all-done.1 = bf16[8,1,96,512]{3,2,1,0:T(8,128)(2,1)S(1)} async-done(((bf16[8,1,96,512]{3,2,1,0:T(8,128)(2,1)}), bf16[8,1,96,512]{3,2,1,0:T(8,128)(2,1)S(1)}, u32[]{:S(2)}, u32[]{:S(2)}) %all-to-all-start.1) | async-done | bytes 786464 | tf_op jit(solution)/shard_map/all_to_all | solution.py:70
  174.0 2.0 %gather_fusion.1 = bf16[512,512]{1,0:T(8,128)(2,1)S(1)} fusion(bf16[768,512]{1,0:T(8,128)(2,1)S(1)} %bitcast.104, s32[1024]{0:T(1024)S(1)} %pad_clamp_fusion), kind=kCustom, calls=%fused_computation.1 | custom fusion | bytes 1050624 | tf_op jit(solution)/shard_map/gather | solution.py:72
  176.0 0.7 reshape.98
  176.6 2.1 %multiply_reduce_fusion = bf16[256,512]{1,0:T(8,128)(2,1)} fusion(f32[256,2,512]{2,1,0:T(2,128)S(1)} %reshape.98, f32[256,2]{1,0:T(8,128)S(1)} %copy.25), kind=kLoop, calls=%fused_computation.27 | loop fusion | flops 393216 | bytes 1312768 | tf_op jit(solution)/shard_map/reduce_sum | solution.py:73
  (17 shorter events, 0.1 us)
Async XLA Ops:
  7.2 109.1 %copy-start = (bf16[256,2048]{1,0:T(8,128)(2,1)S(1)}, bf16[256,2048]{1,0:T(8,128)(2,1)}, u32[]{:S(2)}) copy-start(bf16[256,2048]{1,0:T(8,128)(2,1)} %param.16) | copy-start | bytes 3145732
  7.2 21.9 %all-gather.3.cloned.1.call-start = ((), (), s32[]{:S(2)}) async-start(), calls=%async_computation.5 | async-start | bytes 1310720 | tf_op jit(solution)/shard_map/all_gather | solution.py:40
  7.9 82.5 %all-gather.5.cloned.1.call-start = ((), (), s32[]{:S(2)}) async-start(), calls=%async_computation.6 | async-start | bytes 3932160 | tf_op jit(solution)/shard_map/all_gather | solution.py:64
  63.6 84.8 %reduce-scatter.5.cloned.1.call-start = ((), (), s32[]{:S(2)}) async-start(), calls=%async_computation.7 | async-start | bytes 3932160 | tf_op jit(solution)/shard_map/reduce_scatter | solution.py:69
  110.5 0.9 copy-start.1
  110.5 1.0 copy-start.2
  110.5 4.4 %copy-start.4 = (f32[3,256]{1,0:T(4,128)S(1)}, f32[3,256]{1,0:T(4,128)}, u32[]{:S(2)}) copy-start(f32[3,256]{1,0:T(4,128)} %param.15) | copy-start | bytes 9220
  110.5 5.7 %copy-start.3 = (bf16[256,256]{1,0:T(8,128)(2,1)S(1)}, bf16[256,256]{1,0:T(8,128)(2,1)}, u32[]{:S(2)}) copy-start(bf16[256,256]{1,0:T(8,128)(2,1)} %param.12) | copy-start | bytes 393220
  110.5 43.4 %copy-start.5 = (f32[256,2]{0,1:T(2,128)S(1)}, f32[256,2]{0,1:T(2,128)}, u32[]{:S(2)}) copy-start(f32[256,2]{0,1:T(2,128)} %param.20) | copy-start | bytes 6148
  110.5 68.1 %reduce-scatter.3.cloned.1.call-start = ((), (), s32[]{:S(2)}) async-start(), calls=%async_computation.4 | async-start | bytes 1310720 | tf_op jit(solution)/shard_map/reduce_scatter | solution.py:31
  111.5 4.7 %collective-permute-start = (bf16[2,2,256]{2,1,0:T(2,128)(2,1)S(1)}, bf16[2,2,256]{2,1,0:T(2,128)(2,1)S(1)}, u32[]{:S(2)}, u32[]{:S(2)}) collective-permute-start(bf16[2,2,256]{2,1,0:T(2,128)(2,1)S(1)} %pad_maximum_fusion), channel_id=1, source_target_pairs={{0,4},{4,8},{8,12},{12,16},{16,20},{20,24},{24,28},{1,5},{5,9},{9,... | collective-permute-start | bytes 6152 | tf_op jit(solution)/shard_map/ppermute | solution.py:10
  148.4 25.6 %all-to-all-start.1 = ((bf16[8,1,96,512]{3,2,1,0:T(8,128)(2,1)}), bf16[8,1,96,512]{3,2,1,0:T(8,128)(2,1)S(1)}, u32[]{:S(2)}, u32[]{:S(2)}) async-start(bf16[8,1,96,512]{3,2,1,0:T(8,128)(2,1)} %bitcast.107), calls=%async_computation.3 | async-start | bytes 1572864 | tf_op jit(solution)/shard_map/all_to_all | solution.py:70
Sparse Core Ops, SparseCore 0:
  9.5 19.4 all-gather.2
  63.7 26.6 all-gather.4
  110.7 37.7 reduce-scatter.4
  151.4 24.7 reduce-scatter.2
where the time goes:
time: 186 us; the launch traced here: 185 us
  waiting for transfers between devices  94.3 us (51%)
  blocking collectives  25.9 us (14%)
  matrix products  21.5 us (12%)
  between operations  14 us (8%)
  local copies, waits for them, and re-layouts  13.3 us (7%)
  starting transfers between devices  9.05 us (5%)
  other arithmetic  7.18 us (4%)
    reduce_scatter x1, waiting for transfers between devices, expert_layer(): lax.psum_scatter(down.astype(jnp.bfloat16), 'tp', scatter_dimension=3, ti...  30.7 us
    all_gather x1, waiting for transfers between devices, expert_layer(): arrived = lax.all_gather(landed, 'tp', axis=2, tiled=True)  26.7 us
    all_to_all x1, blocking collectives, expert_layer(): landed = lax.all_to_all(mine, 'ep', split_axis=0, concat_axis=0, tiled=True)  25.9 us
    all_to_all x1, waiting for transfers between devices, expert_layer(): lax.all_to_all(summed, 'ep', split_axis=0, concat_axis=0, tiled=True)  19.9 us
    all_gather x1, waiting for transfers between devices, expert_layer(): whole = lax.all_gather(moe_x, 'tp', axis=1, tiled=True)  15 us
    dot_general x1, matrix products, expert_layer(): jnp.einsum('secf,efd->secd', hidden, w_down, preferred_element_type=jnp.f...  12.1 us
    dot_general x1, matrix products, expert_layer(): jnp.einsum('secd,edf->secf', arrived, w_gate, preferred_element_type=jnp....  8 us
    all_to_all x1, starting transfers between devices, expert_layer(): lax.all_to_all(summed, 'ep', split_axis=0, concat_axis=0, tiled=True)  5.52 us
  transfers between devices with their start and end apart: 6, of which 5 were waited for; matrix products, arithmetic and copies ran while one was open for 7% of the time, Pallas kernels for 0%

commit v1 on v0

--- a/solution.py
+++ b/solution.py
@@ -61,7 +61,15 @@
     part = cap // n_tp
     mine = lax.dynamic_slice_in_dim(outgoing, lax.axis_index("tp") * part, part, 2)
     landed = lax.all_to_all(mine, "ep", split_axis=0, concat_axis=0, tiled=True)
-    arrived = lax.all_gather(landed, "tp", axis=2, tiled=True)
+    devices_2 = lax.axis_size("tp")
+    moving, blocks = (landed, [landed])
+    for _ in range(devices_2 - 1):
+        moving = lax.ppermute(
+            moving, "tp", [(i_2, (i_2 + 1) % devices_2) for i_2 in range(devices_2)]
+        )
+        blocks.insert(0, moving)
+    merged = jnp.concatenate(blocks, axis=2)
+    arrived = jnp.roll(merged, (lax.axis_index("tp") + 1) * landed.shape[2], axis=2)
     gate = jnp.einsum("secd,edf->secf", arrived, w_gate, preferred_element_type=jnp.float32)
     upper = jnp.einsum("secd,edf->secf", arrived, w_up, preferred_element_type=jnp.float32)
     hidden = (jax.nn.silu(gate) * upper).astype(jnp.bfloat16)

time: 186 us -> 194 us (1.043)
  waiting for transfers between devices: 94.3 us -> 101 us
  local copies, waits for them, and re-layouts: 13.3 us -> 18 us
  matrix products: 21.5 us -> 18.6 us
    ppermute x0 -> x3, waiting for transfers between devices: none -> 34.3 us  [expert_layer(): lax.ppermute(moving, 'tp', [(i_2, (i_2 + 1) % devices_2) for i_2 in range...]
    all_gather x1 -> x0, waiting for transfers between devices: 26.7 us -> none  [expert_layer(): arrived = lax.all_gather(landed, 'tp', axis=2, tiled=True)]
    unnamed x14 -> x25, local copies, waits for them, and re-layouts: 1.83 us -> 6.49 us
    dot_general x1, matrix products: 8 us -> 4.92 us  [expert_layer(): jnp.einsum('secd,edf->secf', arrived, w_gate, preferred_element_type=jnp....]
  transfers between devices with their start and end apart: 6 -> 8, of which waited for: 5 -> 7; matrix products, arithmetic and copies ran while one was open for 7% -> 6% of each run, Pallas kernels for 0% -> 0%
where the time goes in v1:
time: 194 us; the launch traced here: 193 us
  waiting for transfers between devices  101 us (52%)
  blocking collectives  25.8 us (13%)
  matrix products  18.6 us (10%)
  local copies, waits for them, and re-layouts  18 us (9%)
  between operations  14 us (7%)
  starting transfers between devices  9 us (5%)
  other arithmetic  7.18 us (4%)
    ppermute x3, waiting for transfers between devices, expert_layer(): lax.ppermute(moving, 'tp', [(i_2, (i_2 + 1) % devices_2) for i_2 in range...  34.3 us
    reduce_scatter x1, waiting for transfers between devices, expert_layer(): lax.psum_scatter(down.astype(jnp.bfloat16), 'tp', scatter_dimension=3, ti...  29.6 us
    all_to_all x1, blocking collectives, expert_layer(): landed = lax.all_to_all(mine, 'ep', split_axis=0, concat_axis=0, tiled=True)  25.8 us
    all_to_all x1, waiting for transfers between devices, expert_layer(): lax.all_to_all(summed, 'ep', split_axis=0, concat_axis=0, tiled=True)  19.9 us
    all_gather x1, waiting for transfers between devices, expert_layer(): whole = lax.all_gather(moe_x, 'tp', axis=1, tiled=True)  15 us
    dot_general x1, matrix products, expert_layer(): jnp.einsum('secf,efd->secd', hidden, w_down, preferred_element_type=jnp.f...  12.2 us
    unnamed x25, local copies, waits for them, and re-layouts  6.49 us
    all_to_all x1, starting transfers between devices, expert_layer(): lax.all_to_all(summed, 'ep', split_axis=0, concat_axis=0, tiled=True)  5.51 us
  transfers between devices with their start and end apart: 8, of which 7 were waited for; matrix products, arithmetic and copies ran while one was open for 6% of the time, Pallas kernels for 0%

profile of v1, /device:TPU:0, one launch (start us, length us, event | category | flops | bytes accessed | tf_op | source)
XLA Modules:
  0.0 193.4 jit_solution(10172168839262738168)
XLA Ops:
  7.2 0.0 all-gather.2.cloned.1.call-start
  7.2 0.7 all-gather.2.cloned.1.call-update
  7.9 0.0 reduce-scatter.5.cloned.1.call-start
  8.0 0.8 copy.20
  8.8 0.1 eq.32
  8.9 0.1 eq.28
  9.1 1.1 reduce-window.6
  10.2 0.2 slice_reduce_fusion
  10.5 0.7 broadcast_multiply_fusion
  11.2 0.1 copy.19
  11.3 0.1 mul.113
  11.5 0.1 fusion.45
  11.6 2.4 %scatter_custom_fusion = s32[768]{0:T(1024)S(1)} fusion(s32[512]{0:T(512)S(1)} %bitcast.106, s32[512]{0:T(512)S(1)} %add_select_fusion, s32[]{:T(128)} %constant.57.clone.1), kind=kCustom, calls=%fused_computation.67 | custom fusion | bytes 3076 | tf_op jit(solution)/shard_map/scatter | solution.py:57
  14.1 15.0 %all-gather.2.cloned.1.call-done = bf16[256,2048]{1,0:T(8,128)(2,1)} async-done(((bf16[256,512]{1,0:T(8,128)(2,1)}), bf16[256,2048]{1,0:T(8,128)(2,1)}) %all-gather.2.cloned.1.call-update) | async-done | bytes 1048592 | tf_op jit(solution)/shard_map/all_gather | solution.py:40
  29.1 1.5 fusion.20
  30.6 1.5 fusion.22
  32.1 0.1 concatenate.17
  32.2 4.3 %gather_fusion = bf16[768,2048]{1,0:T(8,128)(2,1)} fusion(bf16[257,2048]{1,0:T(8,128)(2,1)S(1)} %concatenate.17, s32[1024]{0:T(1024)S(1)} %pad_clamp_fusion.1), kind=kCustom, calls=%fused_computation | custom fusion | bytes 6294528 | tf_op jit(solution)/shard_map/gather | solution.py:60
  36.5 1.2 constant_dynamic-slice_fusion
  37.7 25.8 %all_to_all.10 = bf16[8,1,24,2048]{3,2,1,0:T(8,128)(2,1)S(1)} all-to-all(bf16[8,1,24,2048]{3,2,1,0:T(8,128)(2,1)S(1)} %constant_dynamic-slice_fusion), channel_id=1, replica_groups=mesh['ep'=8,'tp'=4] {'ep'}, dimensions={0} | all-to-all | bytes 1572864 | tf_op jit(solution)/shard_map/all_to_all | solution.py:63
  63.5 11.4 %collective-permute-done.1 = bf16[8,1,24,2048]{3,2,1,0:T(8,128)(2,1)S(1)} collective-permute-done((bf16[8,1,24,2048]{3,2,1,0:T(8,128)(2,1)S(1)}, bf16[8,1,24,2048]{3,2,1,0:T(8,128)(2,1)S(1)}, u32[]{:S(2)}, u32[]{:S(2)}) %collective-permute-start.1) | collective-permute-done | bytes 786464 | tf_op jit(solution)/shard_map/ppermute | solution.py:67
  74.9 11.4 %collective-permute-done.2 = bf16[8,1,24,2048]{3,2,1,0:T(8,128)(2,1)S(1)} collective-permute-done((bf16[8,1,24,2048]{3,2,1,0:T(8,128)(2,1)S(1)}, bf16[8,1,24,2048]{3,2,1,0:T(8,128)(2,1)S(1)}, u32[]{:S(2)}, u32[]{:S(2)}) %collective-permute-start.2) | collective-permute-done | bytes 786464 | tf_op jit(solution)/shard_map/ppermute | solution.py:67
  86.3 11.5 %collective-permute-done.3 = bf16[8,1,24,2048]{3,2,1,0:T(8,128)(2,1)} collective-permute-done((bf16[8,1,24,2048]{3,2,1,0:T(8,128)(2,1)S(1)}, bf16[8,1,24,2048]{3,2,1,0:T(8,128)(2,1)}, u32[]{:S(2)}, u32[]{:S(2)}) %collective-permute-start.3) | collective-permute-done | bytes 786464 | tf_op jit(solution)/shard_map/ppermute | solution.py:67
  97.8 1.2 constant_dynamic-update-slice_fusion.7
  99.0 0.1 constant_dynamic-update-slice_fusion.6
  99.1 0.1 constant_dynamic-update-slice_fusion.5
  99.2 0.1 constant_dynamic-update-slice_fusion.4
  99.3 1.3 constant_dynamic-update-slice_fusion.3
  100.6 0.1 constant_dynamic-update-slice_fusion.2
  100.7 0.1 constant_dynamic-update-slice_fusion.1
  100.8 0.1 constant_dynamic-update-slice_fusion
  100.8 2.6 %copy-done.4 = bf16[8,1,192,2048]{3,2,1,0:T(8,128)(2,1)} copy-done((bf16[8,1,192,2048]{3,2,1,0:T(8,128)(2,1)}, bf16[8,1,192,2048]{3,2,1,0:T(8,128)(2,1)S(1)}, u32[]{:S(2)}) %copy-start.4) | copy-done | bytes 6291480
  103.5 4.9 %fusion.4 = f32[8,96,896]{2,1,0:T(8,128)} fusion(bf16[1,2048,896]{2,1,0:T(8,128)(2,1)S(1)} %copy-done.7, bf16[8,1,192,2048]{3,2,1,0:T(8,128)(2,1)S(1)} %constant_dynamic-update-slice_fusion, s32[]{:T(128)S(6)} %select_n.40), kind=kOutput, calls=%fused_computation.7 | convolution fusion | flops 2818572288 | bytes 9568260 | tf_op jit(solution)/shard_map/secd,edf->secf/dot_general | solution.py:73
  108.4 12.2 %fusion.11 = bf16[8,1,96,2048]{3,2,0,1:T(8,128)(2,1)} fusion(bf16[1,896,2048]{2,1,0:T(8,128)(2,1)} %param.23, bf16[1,2048,896]{2,1,0:T(8,128)(2,1)} %param.22, bf16[8,1,192,2048]{3,2,1,0:T(8,128)(2,1)} %copy-done.4, s32[]{:T(128)S(6)} %select_n.40, f32[8,96,896]{2,1,0:T(8,128)} %fusion.4), kind=kOutput, calls=%fused_computation.12 | convolution fusion | flops 5642846208 | bytes 16384004 | tf_op jit(solution)/shard_map/secf,efd->secd/dot_general | solution.py:76
  120.6 0.0 reduce-scatter.5.cloned.1.call-update
  120.7 0.0 reduce-scatter.3.cloned.1.call-start
  120.8 3.4 %collective-permute-start = (bf16[2,2,256]{2,1,0:T(2,128)(2,1)S(1)}, bf16[2,2,256]{2,1,0:T(2,128)(2,1)S(1)}, u32[]{:S(2)}, u32[]{:S(2)}) collective-permute-start(bf16[2,2,256]{2,1,0:T(2,128)(2,1)S(1)} %pad_maximum_fusion), channel_id=1, source_target_pairs={{0,4},{4,8},{8,12},{12,16},{16,20},{20,24},{24,28},{1,5},{5,9},{9,... | collective-permute-start | bytes 6152 | tf_op jit(solution)/shard_map/ppermute | solution.py:10
  124.2 1.3 collective-permute-done
  125.4 0.1 convert_multiply_fusion.2
  125.5 1.5 convolution_convert_fusion
  127.0 0.0 reduce-scatter.3.cloned.1.call-update
  127.0 29.6 %reduce-scatter.5.cloned.1.call-done = bf16[8,1,96,512]{3,2,0,1:T(8,128)(2,1)} async-done(((bf16[8,1,96,2048]{3,2,0,1:T(8,128)(2,1)}), bf16[8,1,96,512]{3,2,0,1:T(8,128)(2,1)}) %reduce-scatter.5.cloned.1.call-update) | async-done | bytes 786448 | tf_op jit(solution)/shard_map/reduce_scatter | solution.py:77
  156.7 5.5 %all-to-all-start.1 = ((bf16[8,1,96,512]{3,2,1,0:T(8,128)(2,1)}), bf16[8,1,96,512]{3,2,1,0:T(8,128)(2,1)S(1)}, u32[]{:S(2)}, u32[]{:S(2)}) async-start(bf16[8,1,96,512]{3,2,1,0:T(8,128)(2,1)} %bitcast.105), calls=%async_computation.3 | async-start | bytes 1572864 | tf_op jit(solution)/shard_map/all_to_all | solution.py:78
  162.2 0.1 copy.24
  162.3 19.9 %all-to-all-done.1 = bf16[8,1,96,512]{3,2,1,0:T(8,128)(2,1)S(1)} async-done(((bf16[8,1,96,512]{3,2,1,0:T(8,128)(2,1)}), bf16[8,1,96,512]{3,2,1,0:T(8,128)(2,1)S(1)}, u32[]{:S(2)}, u32[]{:S(2)}) %all-to-all-start.1) | async-done | bytes 786464 | tf_op jit(solution)/shard_map/all_to_all | solution.py:78
  182.2 2.0 %gather_fusion.1 = bf16[512,512]{1,0:T(8,128)(2,1)S(1)} fusion(bf16[768,512]{1,0:T(8,128)(2,1)S(1)} %bitcast.103, s32[1024]{0:T(1024)S(1)} %pad_clamp_fusion), kind=kCustom, calls=%fused_computation.1 | custom fusion | bytes 1050624 | tf_op jit(solution)/shard_map/gather | solution.py:80
  184.2 0.7 reshape.98
  184.9 2.1 %multiply_reduce_fusion = bf16[256,512]{1,0:T(8,128)(2,1)} fusion(f32[256,2,512]{2,1,0:T(2,128)S(1)} %reshape.98, f32[256,2]{1,0:T(8,128)S(1)} %copy.24), kind=kLoop, calls=%fused_computation.29 | loop fusion | flops 393216 | bytes 1312768 | tf_op jit(solution)/shard_map/reduce_sum | solution.py:81
  (32 shorter events, 0.2 us)
Async XLA Ops:
  7.2 118.3 %copy-start = (bf16[256,2048]{1,0:T(8,128)(2,1)S(1)}, bf16[256,2048]{1,0:T(8,128)(2,1)}, u32[]{:S(2)}) copy-start(bf16[256,2048]{1,0:T(8,128)(2,1)} %param.16) | copy-start | bytes 3145732
  7.2 21.9 %all-gather.2.cloned.1.call-start = ((), (), s32[]{:S(2)}) async-start(), calls=%async_computation.5 | async-start | bytes 1310720 | tf_op jit(solution)/shard_map/all_gather | solution.py:40
  7.9 148.7 %reduce-scatter.5.cloned.1.call-start = ((), (), s32[]{:S(2)}) async-start(), calls=%async_computation.6 | async-start | bytes 3932160 | tf_op jit(solution)/shard_map/reduce_scatter | solution.py:77
  63.5 11.4 %collective-permute-start.1 = (bf16[8,1,24,2048]{3,2,1,0:T(8,128)(2,1)S(1)}, bf16[8,1,24,2048]{3,2,1,0:T(8,128)(2,1)S(1)}, u32[]{:S(2)}, u32[]{:S(2)}) collective-permute-start(bf16[8,1,24,2048]{3,2,1,0:T(8,128)(2,1)S(1)} %all_to_all.10), channel_id=1, source_target_pairs={{0,1},{1,2},{2,3},{3,0},{4,5},{5,6},{6,7},{7,4},{8,9},{9,10},{10,1... | collective-permute-start | bytes 2359304 | tf_op jit(solution)/shard_map/ppermute | solution.py:67
  74.9 11.4 %collective-permute-start.2 = (bf16[8,1,24,2048]{3,2,1,0:T(8,128)(2,1)S(1)}, bf16[8,1,24,2048]{3,2,1,0:T(8,128)(2,1)S(1)}, u32[]{:S(2)}, u32[]{:S(2)}) collective-permute-start(bf16[8,1,24,2048]{3,2,1,0:T(8,128)(2,1)S(1)} %collective-permute-done.1), channel_id=1, source_target_pairs={{0,1},{1,2},{2,3},{3,0},{4,5},{5,6},{6,7},{7,4},{8,9},{9,10},{10,1... | collective-permute-start | bytes 2359304 | tf_op jit(solution)/shard_map/ppermute | solution.py:67
  86.3 11.5 %collective-permute-start.3 = (bf16[8,1,24,2048]{3,2,1,0:T(8,128)(2,1)S(1)}, bf16[8,1,24,2048]{3,2,1,0:T(8,128)(2,1)}, u32[]{:S(2)}, u32[]{:S(2)}) collective-permute-start(bf16[8,1,24,2048]{3,2,1,0:T(8,128)(2,1)S(1)} %collective-permute-done.2), channel_id=1, source_target_pairs={{0,1},{1,2},{2,3},{3,0},{4,5},{5,6},{6,7},{7,4},{8,9},{9,10},{10,1... | collective-permute-start | bytes 2359304 | tf_op jit(solution)/shard_map/ppermute | solution.py:67
  99.2 4.3 %copy-start.7 = (bf16[1,2048,896]{2,1,0:T(8,128)(2,1)S(1)}, bf16[1,2048,896]{2,1,0:T(8,128)(2,1)}, u32[]{:S(2)}) copy-start(bf16[1,2048,896]{2,1,0:T(8,128)(2,1)} %param.21) | copy-start | bytes 11010052
  100.8 2.7 %copy-start.4 = (bf16[8,1,192,2048]{3,2,1,0:T(8,128)(2,1)}, bf16[8,1,192,2048]{3,2,1,0:T(8,128)(2,1)S(1)}, u32[]{:S(2)}) copy-start(bf16[8,1,192,2048]{3,2,1,0:T(8,128)(2,1)S(1)} %constant_dynamic-update-slice_fusion) | copy-start | bytes 18874372
  108.4 12.3 %copy-start.1 = (bf16[256,256]{1,0:T(8,128)(2,1)S(1)}, bf16[256,256]{1,0:T(8,128)(2,1)}, u32[]{:S(2)}) copy-start(bf16[256,256]{1,0:T(8,128)(2,1)} %param.13) | copy-start | bytes 393220
  108.4 12.3 %copy-start.2 = (bf16[256,256]{1,0:T(8,128)(2,1)S(1)}, bf16[256,256]{1,0:T(8,128)(2,1)}, u32[]{:S(2)}) copy-start(bf16[256,256]{1,0:T(8,128)(2,1)} %param.14) | copy-start | bytes 393220
  108.4 15.7 %copy-start.5 = (f32[3,256]{1,0:T(4,128)S(1)}, f32[3,256]{1,0:T(4,128)}, u32[]{:S(2)}) copy-start(f32[3,256]{1,0:T(4,128)} %param.15) | copy-start | bytes 9220
  120.6 4.9 %copy-start.3 = (bf16[256,256]{1,0:T(8,128)(2,1)S(1)}, bf16[256,256]{1,0:T(8,128)(2,1)}, u32[]{:S(2)}) copy-start(bf16[256,256]{1,0:T(8,128)(2,1)} %param.12) | copy-start | bytes 393220
  120.6 41.5 %copy-start.6 = (f32[256,2]{0,1:T(2,128)S(1)}, f32[256,2]{0,1:T(2,128)}, u32[]{:S(2)}) copy-start(f32[256,2]{0,1:T(2,128)} %param.20) | copy-start | bytes 6148
  120.7 66.2 %reduce-scatter.3.cloned.1.call-start = ((), (), s32[]{:S(2)}) async-start(), calls=%async_computation.4 | async-start | bytes 1310720 | tf_op jit(solution)/shard_map/reduce_scatter | solution.py:31
  120.8 4.7 %collective-permute-start = (bf16[2,2,256]{2,1,0:T(2,128)(2,1)S(1)}, bf16[2,2,256]{2,1,0:T(2,128)(2,1)S(1)}, u32[]{:S(2)}, u32[]{:S(2)}) collective-permute-start(bf16[2,2,256]{2,1,0:T(2,128)(2,1)S(1)} %pad_maximum_fusion), channel_id=1, source_target_pairs={{0,4},{4,8},{8,12},{12,16},{16,20},{20,24},{24,28},{1,5},{5,9},{9,... | collective-permute-start | bytes 6152 | tf_op jit(solution)/shard_map/ppermute | solution.py:10
  156.7 25.6 %all-to-all-start.1 = ((bf16[8,1,96,512]{3,2,1,0:T(8,128)(2,1)}), bf16[8,1,96,512]{3,2,1,0:T(8,128)(2,1)S(1)}, u32[]{:S(2)}, u32[]{:S(2)}) async-start(bf16[8,1,96,512]{3,2,1,0:T(8,128)(2,1)} %bitcast.105), calls=%async_computation.3 | async-start | bytes 1572864 | tf_op jit(solution)/shard_map/all_to_all | solution.py:78
Sparse Core Ops, SparseCore 0:
  9.5 19.4 all-gather.1
  120.8 35.8 reduce-scatter.4
  159.8 24.8 reduce-scatter.2
